TPU v7x, 32 devices: a whole 2x2x4 slice. The times are simulated.
32 devices in a mesh: kv: 8 (over z, x), tp: 4 (over y, core).
Axes of the slice: x: 2, y: 2, z: 4, core: 2. Of those that a mesh axis runs over, the one named last changes fastest.
Arguments:
- hidden: bfloat16 [128, 4, 2048], P(None, None, 'kv'), may hold values from -18 to 18
- norm_gain: float32 [2048], replicated, may hold values from 0.1 to 1.9
- w_query: bfloat16 [2048, 1024], P(None, 'tp'), may hold values from -0.125 to 0.125
- w_forget: bfloat16 [2048, 1024], P(None, 'tp'), may hold values from -0.125 to 0.125
- w_input: bfloat16 [2048, 1024], P(None, 'tp'), may hold values from -0.125 to 0.125
- w_outgate: bfloat16 [2048, 1024], P(None, 'tp'), may hold values from -0.125 to 0.125
- w_out: bfloat16 [1024, 2048], replicated, may hold values from -0.1875 to 0.1875
- floor: float32 [1024], P('tp'), may hold values from 0 to 0.95
- head_gain: float32 [128], replicated, may hold values from 0.1 to 1.9
- base_state: float32 [128, 8, 128, 128], P('kv', 'tp'), may hold values from -4 to 4
- prev_forget: bfloat16 [128, 4, 1024], P('kv', None, 'tp'), may hold values from -6 to 6
- prev_input: bfloat16 [128, 4, 1024], P('kv', None, 'tp'), may hold values from -6 to 6
- accepted: int32 [128], P('kv'), may hold values from 0 to 4
Outputs:
- mixed: bfloat16 [128, 4, 2048], P(None, None, 'kv')
- taken_state: float32 [128, 8, 128, 128], P('kv', 'tp')
All inputs are finite; a program needn't handle non-finite values.
Results may differ from a plain program's by a relative error of at most 0.014.
Values may be sent and summed in bfloat16 or wider, within the bound.
A program may use at most 64 MiB of HBM per device.

v0:
```python
import jax
import jax.numpy as jnp
from jax import lax
from jax.sharding import PartitionSpec as P

D = 2048
HEAD_DIM = 128
PROPS = 4


def shards(
    hidden,
    norm_gain,
    w_query,
    w_forget,
    w_input,
    w_outgate,
    w_out,
    floor,
    head_gain,
    base_state,
    prev_forget,
    prev_input,
    accepted,
):
    arrived = lax.all_to_all(hidden, "kv", split_axis=0, concat_axis=2, tiled=True)
    whole_vals = arrived.astype(jnp.float32)
    row_sums = jnp.sum(whole_vals * whole_vals, axis=2)
    normed = (whole_vals * lax.rsqrt(row_sums / D + 1e-06)[..., None] * norm_gain).astype(
        jnp.bfloat16
    )
    query_pre = jnp.dot(normed, w_query, preferred_element_type=jnp.float32).astype(jnp.bfloat16)
    forget_pre = jnp.dot(normed, w_forget, preferred_element_type=jnp.float32).astype(jnp.bfloat16)
    input_pre = jnp.dot(normed, w_input, preferred_element_type=jnp.float32).astype(jnp.bfloat16)
    gate_pre = jnp.dot(normed, w_outgate, preferred_element_type=jnp.float32).astype(jnp.bfloat16)
    seq_local = normed.shape[0]
    head_local = w_query.shape[1] // HEAD_DIM
    shape = (seq_local, PROPS, head_local, HEAD_DIM)
    query = jax.nn.silu(query_pre.astype(jnp.float32)).reshape(shape)
    forget = (floor + (1.0 - floor) * jax.nn.sigmoid(forget_pre.astype(jnp.float32))).reshape(shape)
    value = input_pre.astype(jnp.float32).reshape(shape)
    prev_f = (floor + (1.0 - floor) * jax.nn.sigmoid(prev_forget.astype(jnp.float32))).reshape(
        shape
    )
    prev_v = prev_input.astype(jnp.float32).reshape(shape)
    state = base_state
    for step in range(PROPS):
        live = (step < accepted)[:, None, None, None]
        moved = (
            prev_f[:, step][..., None] * state
            + (1.0 - prev_f[:, step])[..., None] * prev_v[:, step][:, :, None, :]
        )
        state = jnp.where(live, moved, state)
    taken_state = state
    outputs = []
    for step in range(PROPS):
        state = (
            forget[:, step][..., None] * state
            + (1.0 - forget[:, step])[..., None] * value[:, step][:, :, None, :]
        )
        outputs.append(
            jnp.einsum("bhk,bhkv->bhv", query[:, step], state, precision=lax.Precision.HIGHEST)
        )
    result = jnp.stack(outputs, axis=1)
    scaled = (
        result * lax.rsqrt(jnp.mean(result * result, axis=-1, keepdims=True) + 1e-05) * head_gain
    )
    gated = scaled * jax.nn.silu(gate_pre.astype(jnp.float32)).reshape(shape)
    mixed_heads = gated.reshape(seq_local, PROPS, head_local * HEAD_DIM).astype(jnp.bfloat16)
    own_rows = mixed_heads.shape[2]
    w_rows = lax.dynamic_slice_in_dim(w_out, lax.axis_index("tp") * own_rows, own_rows, 0)
    partial_value = jnp.dot(mixed_heads, w_rows, preferred_element_type=jnp.float32)
    finished = lax.psum(partial_value, "tp").astype(jnp.bfloat16)
    mixed = lax.all_to_all(finished, "kv", split_axis=2, concat_axis=0, tiled=True)
    return (mixed, taken_state)


def solution(mesh):
    placed = (
        P(None, None, "kv"),
        P(),
        P(None, "tp"),
        P(None, "tp"),
        P(None, "tp"),
        P(None, "tp"),
        P(),
        P("tp"),
        P(),
        P("kv", "tp", None, None),
        P("kv", None, "tp"),
        P("kv", None, "tp"),
        P("kv"),
    )
    return jax.shard_map(
        shards,
        mesh=mesh,
        in_specs=placed,
        out_specs=(P(None, None, "kv"), P("kv", "tp", None, None)),
        check_vma=False,
    )
```

profile of v0, /device:TPU:0, one launch (start us, length us, event | category | flops | bytes accessed | tf_op | source)
XLA Modules:
  0.0 96.0 jit_solution(18002514994027775703)
XLA Ops:
  0.6 7.4 %all-to-all-start = ((bf16[128,4,256]{2,1,0:T(4,128)(2,1)}), bf16[128,4,256]{2,1,0:T(4,128)(2,1)S(1)}, u32[]{:S(2)}, u32[]{:S(2)}) async-start(bf16[128,4,256]{2,1,0:T(4,128)(2,1)} %param.13), calls=%async_computation | async-start | bytes 524288 | tf_op jit(solution)/shard_map/all_to_all | solution.py:26
  8.1 0.7 broadcast_subtract_fusion.8
  8.8 0.6 copy-done.3
  9.3 0.8 multiply_add_fusion.9
  10.2 1.2 %broadcast_bitcast_fusion = f32[256]{0:T(256)} fusion(f32[128]{0:T(128)} %param.21), kind=kLoop, calls=%fused_computation.82 | loop fusion | bytes 1536 | tf_op jit(solution)/shard_map/mul | solution.py:66
  11.5 1.3 %broadcast_compare_fusion.3 = (pred[16]{0:T(512)(128)(4,1)}, pred[16]{0:T(512)(128)(4,1)}, pred[16]{0:T(512)(128)(4,1)}, pred[16]{0:T(512)(128)(4,1)}) fusion(s32[16]{0:T(128)} %param.25), kind=kLoop, calls=%fused_computation.88 | loop fusion | flops 64 | bytes 128 | tf_op jit(solution)/shard_map/gt | solution.py:48
  12.7 0.8 reshape.130
  13.5 0.6 slice_bitcast_fusion.10
  14.1 7.1 %add_select_fusion = f32[16,2,128,128]{3,2,1,0:T(8,128)S(1)} fusion(f32[16,2,128,128]{3,2,1,0:T(8,128)} %param.22, f32[16,2,128]{2,1,0:T(2,128)} %get-tuple-element.29, f32[16,2,128]{2,1,0:T(2,128)S(1)} %get-tuple-element.25, f32[16,2,128]{2,1,0:T(2,128)} %get-tuple-element.27, f32[16,2,128]{2,1,0:T(2,128)S(1)} %get-tuple-element.24, ...), kind=kLoop, calls=%fused_computation.7 | loop fusion | flops 8388608 | bytes 4390976 | tf_op jit(solution)/shard_map/jit(_where)/select_n | solution.py:53
  21.3 0.2 multiply_reduce_fusion
  21.7 1.1 %copy.38 = f32[16,4,8,256]{3,2,0,1:T(8,128)} copy(f32[16,4,8,256]{3,1,0,2:T(4,128)S(1)} %bitcast.141) | data formatting | bytes 1048576 | tf_op jit(solution)/shard_map/convert_element_type | solution.py:27
  22.8 1.9 %reshape.128 = f32[16,4,2048]{2,0,1:T(8,128)} reshape(f32[16,4,8,256]{3,2,0,1:T(8,128)} %copy.38) | data formatting | bytes 1048576 | tf_op jit(solution)/shard_map/convert_element_type | solution.py:27
  24.8 1.2 %multiply_convert_fusion = bf16[16,4,2048]{2,0,1:T(8,128)(2,1)S(1)} fusion(f32[16,4,2048]{2,0,1:T(8,128)} %reshape.128, f32[2048]{0:T(1024)S(1)} %copy-done.5, f32[16,4]{0,1:T(4,128)S(1)} %add_rsqrt_fusion.1), kind=kLoop, calls=%fused_computation.43 | loop fusion | flops 393216 | bytes 794880 | tf_op jit(solution)/shard_map/convert_element_type | solution.py:29
  25.9 1.5 %fusion.14 = f32[16,4,256]{2,0,1:T(8,128)S(1)} fusion(bf16[16,4,2048]{2,0,1:T(8,128)(2,1)S(1)} %multiply_convert_fusion, bf16[2048,256]{1,0:T(8,128)(2,1)} %param.16, f32[256]{0:T(256)S(1)} %copy-done.4, f32[256]{0:T(256)S(1)} %copy-done.2), kind=kOutput, calls=%fused_computation.21 | convolution fusion | flops 67223552 | bytes 1378304 | tf_op jit(solution)/shard_map/dot_general | solution.py:33
  27.5 1.5 %fusion.7 = f32[16,4,256]{2,0,1:T(8,128)S(1)} fusion(bf16[16,4,2048]{2,0,1:T(8,128)(2,1)S(1)} %multiply_convert_fusion, bf16[2048,256]{1,0:T(8,128)(2,1)} %param.17), kind=kOutput, calls=%fused_computation.13 | convolution fusion | flops 67141632 | bytes 1376256 | tf_op jit(solution)/shard_map/dot_general | solution.py:34
  29.1 0.7 reshape.132
  29.7 2.2 %divide_multiply_fusion = f32[16,4,256]{2,0,1:T(8,128)} fusion(bf16[16,4,2048]{2,0,1:T(8,128)(2,1)S(1)} %multiply_convert_fusion, bf16[2048,256]{1,0:T(8,128)(2,1)} %param.15), kind=kOutput, calls=%fused_computation.53 | convolution fusion | flops 67207168 | bytes 1376256 | tf_op jit(solution)/shard_map/dot_general | solution.py:32
  31.9 0.9 reshape.121
  32.8 0.8 slice_bitcast_fusion.6
  33.6 2.8 %fusion.4 = f32[16,2,1,128]{3,2,1,0:T(1,128)S(1)} fusion(f32[16,2,128,1]{2,3,1,0:T(1,128)S(1)} %bitcast.146, f32[16,2,128,128]{3,2,1,0:T(8,128)S(1)} %add_select_fusion, f32[16,2,128]{2,1,0:T(2,128)S(1)} %get-tuple-element.14, f32[16,2,128]{2,1,0:T(2,128)S(1)} %get-tuple-element.10, f32[16,2,128]{2,1,0:T(2,128)S(1)} %get-tuple-element.37), kind=kOutput, calls=%fused_computation.8 | convolution fusion | flops 7864320 | bytes 2179072 | tf_op jit(solution)/shard_map/bhk,bhkv->bhv/dot_general | solution.py:62
  36.4 4.3 %fusion.35 = f32[16,2,1,128]{3,2,1,0:T(1,128)S(1)} fusion(f32[16,2,128,1]{2,3,1,0:T(1,128)S(1)} %bitcast.155, f32[16,2,128,128]{3,2,1,0:T(8,128)S(1)} %add_select_fusion, f32[16,2,128]{2,1,0:T(2,128)S(1)} %get-tuple-element.17, f32[16,2,128]{2,1,0:T(2,128)S(1)} %get-tuple-element.13, f32[16,2,128]{2,1,0:T(2,128)S(1)} %get-tuple-element.34, ...), kind=kOutput, calls=%fused_computation.45 | convolution fusion | flops 9437184 | bytes 2228224 | tf_op jit(solution)/shard_map/bhk,bhkv->bhv/dot_general | solution.py:62
  40.7 6.1 %fusion.5 = f32[16,2,1,128]{3,2,1,0:T(1,128)S(1)} fusion(f32[16,2,128,1]{2,3,1,0:T(1,128)S(1)} %bitcast.154, f32[16,2,128]{2,1,0:T(2,128)S(1)} %get-tuple-element.16, f32[16,2,128]{2,1,0:T(2,128)S(1)} %get-tuple-element.12, f32[16,2,128]{2,1,0:T(2,128)S(1)} %get-tuple-element.35, f32[16,2,128,128]{3,2,1,0:T(8,128)S(1)} %add_select_fusion, ...), kind=kOutput, calls=%fused_computation.9 | convolution fusion | flops 11010048 | bytes 2277376 | tf_op jit(solution)/shard_map/bhk,bhkv->bhv/dot_general | solution.py:62
  46.8 7.2 %fusion = f32[16,2,1,128]{3,2,1,0:T(1,128)S(1)} fusion(f32[16,2,128,1]{2,3,1,0:T(1,128)S(1)} %bitcast.153, f32[16,2,128]{2,1,0:T(2,128)S(1)} %get-tuple-element.15, f32[16,2,128]{2,1,0:T(2,128)S(1)} %get-tuple-element.11, f32[16,2,128]{2,1,0:T(2,128)S(1)} %get-tuple-element.36, f32[16,2,128]{2,1,0:T(2,128)S(1)} %get-tuple-element.16, ...), kind=kOutput, calls=%fused_computation | convolution fusion | flops 12582912 | bytes 2326528 | tf_op jit(solution)/shard_map/bhk,bhkv->bhv/dot_general | solution.py:62
  54.1 0.1 fusion.39
  54.2 0.1 mul.343
  54.4 2.0 %fusion.16 = f32[16,4,2048]{2,0,1:T(8,128)S(1)} fusion(bf16[1024,2048]{1,0:T(8,128)(2,1)} %param.19, s32[]{:T(128)S(6)} %select_n.20, f32[16,4,256]{2,0,1:T(8,128)S(1)} %mul.344, f32[16,1,256]{2,0,1:T(8,128)S(1)} %stack.28, f32[16,1,256]{2,0,1:T(8,128)S(1)} %stack.27, f32[16,1,256]{2,0,1:T(8,128)S(1)} %stack.26, f32[16,1,256]{2,0,1:T(8,128)S(1)} %stack.25, ...), kind=kOutput, calls=%fused_computation.24 | convolution fusion | flops 134430720 | bytes 3015684 | tf_op jit(solution)/shard_map/dot_general | solution.py:72
  56.5 16.6 %all-reduce.1 = bf16[16,4,2048]{2,0,1:T(8,128)(2,1)S(1)} all-reduce(f32[16,4,2048]{2,0,1:T(8,128)S(1)} %fusion.16), channel_id=1, replica_groups=mesh['kv'=8,'tp'=4] {'tp'}, use_global_device_ids=true, to_apply=%region_3.4 | all-reduce | flops 131072 | bytes 786432 | tf_op jit(solution)/shard_map/psum | solution.py:73
  73.1 1.4 %copy.45 = bf16[16,4,2048]{0,1,2:T(4,128)(2,1)S(1)} copy(bf16[16,4,2048]{2,0,1:T(8,128)(2,1)S(1)} %all-reduce.1) | data formatting | bytes 524288 | tf_op jit(solution)/shard_map/convert_element_type | solution.py:73
  74.5 2.2 %reshape.148 = bf16[8,2,8192]{2,1,0:T(2,128)(2,1)S(1)} reshape(bf16[2048,4,16]{2,1,0:T(4,128)(2,1)S(1)} %bitcast.139) | data formatting | bytes 524288
  76.7 14.9 %all_to_all.27 = bf16[8,2,8192]{2,1,0:T(2,128)(2,1)} all-to-all(bf16[8,2,8192]{2,1,0:T(2,128)(2,1)S(1)} %reshape.148), channel_id=1, replica_groups=mesh['kv'=8,'tp'=4] {'kv'}, dimensions={0} | all-to-all | bytes 524288 | tf_op jit(solution)/shard_map/all_to_all | solution.py:74
  91.5 2.4 %reshape.149 = bf16[2048,4,16]{2,1,0:T(4,128)(2,1)S(1)} reshape(bf16[8,2,8192]{2,1,0:T(2,128)(2,1)} %all_to_all.27) | data formatting | bytes 524288
  94.0 2.0 %copy.46 = bf16[8,16,4,256]{3,2,1,0:T(4,128)(2,1)} copy(bf16[8,16,4,256]{1,2,3,0:T(4,128)(2,1)S(1)} %bitcast.140) | data formatting | bytes 524288 | tf_op jit(solution)/shard_map/all_to_all | solution.py:74
  (30 shorter events, 0.5 us)
Async XLA Ops:
  0.6 53.8 %copy-start = (bf16[2048,256]{1,0:T(8,128)(2,1)S(1)}, bf16[2048,256]{1,0:T(8,128)(2,1)}, u32[]{:S(2)}) copy-start(bf16[2048,256]{1,0:T(8,128)(2,1)} %param.18) | copy-start | bytes 3145732
  0.6 20.7 %all-to-all-start = ((bf16[128,4,256]{2,1,0:T(4,128)(2,1)}), bf16[128,4,256]{2,1,0:T(4,128)(2,1)S(1)}, u32[]{:S(2)}, u32[]{:S(2)}) async-start(bf16[128,4,256]{2,1,0:T(4,128)(2,1)} %param.13), calls=%async_computation | async-start | bytes 524288 | tf_op jit(solution)/shard_map/all_to_all | solution.py:26
  8.8 0.6 copy-start.3
  21.3 25.5 %copy-start.1 = (f32[16,2,128,128]{3,2,1,0:T(8,128)}, f32[16,2,128,128]{3,2,1,0:T(8,128)S(1)}, u32[]{:S(2)}) copy-start(f32[16,2,128,128]{3,2,1,0:T(8,128)S(1)} %add_select_fusion) | copy-start | bytes 6291460
  21.3 3.5 %copy-start.5 = (f32[2048]{0:T(1024)S(1)}, f32[2048]{0:T(1024)}, u32[]{:S(2)}) copy-start(f32[2048]{0:T(1024)} %param.14) | copy-start | bytes 24580
  21.3 4.6 %copy-start.2 = (f32[256]{0:T(256)S(1)}, f32[256]{0:T(256)}, u32[]{:S(2)}) copy-start(f32[256]{0:T(256)} %param.20) | copy-start | bytes 3076
  21.3 4.6 %copy-start.4 = (f32[256]{0:T(256)S(1)}, f32[256]{0:T(256)}, u32[]{:S(2)}) copy-start(f32[256]{0:T(256)} %copy-done.3) | copy-start | bytes 3076
  46.8 7.7 %copy-start.6 = (f32[256]{0:T(256)S(1)}, f32[256]{0:T(256)}, u32[]{:S(2)}) copy-start(f32[256]{0:T(256)} %broadcast_bitcast_fusion) | copy-start | bytes 3076
where the time goes:
time: 96.9 us; the launch traced here: 96 us
  blocking collectives  31.5 us (33%)
  matrix products  27.6 us (28%)
  local copies, waits for them, and re-layouts  17 us (18%)
  other arithmetic  11.5 us (12%)
  starting transfers between devices  7.42 us (8%)
    dot_general x4, matrix products, shards(): jnp.einsum('bhk,bhkv->bhv', query[:, step], state, precision=lax.Precisio...  20.3 us
    psum x1, blocking collectives, shards(): finished = lax.psum(partial_value, 'tp').astype(jnp.bfloat16)  16.6 us
    all_to_all x1, blocking collectives, shards(): lax.all_to_all(finished, 'kv', split_axis=2, concat_axis=0, tiled=True)  14.9 us
    all_to_all x1, starting transfers between devices, shards(): lax.all_to_all(hidden, 'kv', split_axis=0, concat_axis=2, tiled=True)  7.42 us
    select_n x1, other arithmetic, shards(): state = jnp.where(live, moved, state)  7.13 us
    unnamed x17, local copies, waits for them, and re-layouts  5.27 us
    convert_element_type x2, local copies, waits for them, and re-layouts, shards(): whole_vals = arrived.astype(jnp.float32)  3.03 us
    dot_general x1, matrix products, shards(): jnp.dot(normed, w_query, preferred_element_type=jnp.float32)  2.17 us
  transfers between devices with their start and end apart: 1, of which 0 were waited for; matrix products, arithmetic and copies ran while one was open for 13% of the time, Pallas kernels for 0%

commit v1 on v0

--- a/solution.py
+++ b/solution.py
@@ -2,6 +2,7 @@
 import jax.numpy as jnp
 from jax import lax
 from jax.sharding import PartitionSpec as P
+from jax.lax import all_to_all, axis_size
 
 D = 2048
 HEAD_DIM = 128
@@ -23,7 +24,15 @@
     prev_input,
     accepted,
 ):
-    arrived = lax.all_to_all(hidden, "kv", split_axis=0, concat_axis=2, tiled=True)
+    arrived = jnp.concatenate(
+        all_to_all(
+            jnp.stack(jnp.split(hidden, axis_size("kv"), axis=0)),
+            axis_name="kv",
+            split_axis=0,
+            concat_axis=0,
+        ),
+        axis=2,
+    )
     whole_vals = arrived.astype(jnp.float32)
     row_sums = jnp.sum(whole_vals * whole_vals, axis=2)
     normed = (whole_vals * lax.rsqrt(row_sums / D + 1e-06)[..., None] * norm_gain).astype(

time: 96.9 us -> 108 us (1.11)
  local copies, waits for them, and re-layouts: 17 us -> 28.1 us
    unnamed x17 -> x23, local copies, waits for them, and re-layouts: 5.27 us -> 15 us
    another operation x0 -> x1, local copies, waits for them, and re-layouts: none -> 1.38 us  [shards(): jnp.stack(jnp.split(hidden, axis_size('kv'), axis=0))]
  transfers between devices with their start and end apart: 1 -> 1, of which waited for: 0 -> 0; matrix products, arithmetic and copies ran while one was open for 13% -> 12% of each run, Pallas kernels for 0% -> 0%
where the time goes in v1:
time: 108 us; the launch traced here: 107 us
  blocking collectives  31.5 us (29%)
  local copies, waits for them, and re-layouts  28.1 us (26%)
  matrix products  27.6 us (26%)
  other arithmetic  11.5 us (11%)
  starting transfers between devices  7.28 us (7%)
    dot_general x4, matrix products, shards(): jnp.einsum('bhk,bhkv->bhv', query[:, step], state, precision=lax.Precisio...  20.3 us
    psum x1, blocking collectives, shards(): finished = lax.psum(partial_value, 'tp').astype(jnp.bfloat16)  16.6 us
    unnamed x23, local copies, waits for them, and re-layouts  15 us
    all_to_all x1, blocking collectives, shards(): lax.all_to_all(finished, 'kv', split_axis=2, concat_axis=0, tiled=True)  14.9 us
    all_to_all x1, starting transfers between devices, shards(): all_to_all(jnp.stack(jnp.split(hidden, axis_size('kv'), axis=0)), axis_na...  7.28 us
    select_n x1, other arithmetic, shards(): state = jnp.where(live, moved, state)  7.13 us
    convert_element_type x2, local copies, waits for them, and re-layouts, shards(): whole_vals = arrived.astype(jnp.float32)  3.01 us
    dot_general x1, matrix products, shards(): jnp.dot(normed, w_query, preferred_element_type=jnp.float32)  2.17 us
  transfers between devices with their start and end apart: 1, of which 0 were waited for; matrix products, arithmetic and copies ran while one was open for 12% of the time, Pallas kernels for 0%

profile of v1, /device:TPU:0, one launch (start us, length us, event | category | flops | bytes accessed | tf_op | source)
XLA Modules:
  0.0 107.0 jit_solution(11793273186378179741)
XLA Ops:
  0.6 1.5 %bitcast_dynamic-update-slice_fusion.7 = bf16[8,16,4,256]{3,2,1,0:T(4,128)(2,1)} fusion(bf16[128,4,256]{2,1,0:T(4,128)(2,1)} %param.13), kind=kLoop, calls=%fused_computation.63 | loop fusion | bytes 65536
  2.1 1.4 %bitcast_dynamic-update-slice_fusion.6 = bf16[8,16,4,256]{3,2,1,0:T(4,128)(2,1)} fusion(bf16[8,16,4,256]{3,2,1,0:T(4,128)(2,1)} %bitcast_dynamic-update-slice_fusion.7, bf16[128,4,256]{2,1,0:T(4,128)(2,1)} %param.13), kind=kLoop, calls=%fused_computation.62 | loop fusion | bytes 65536
  3.5 1.4 %bitcast_dynamic-update-slice_fusion.5 = bf16[8,16,4,256]{3,2,1,0:T(4,128)(2,1)} fusion(bf16[8,16,4,256]{3,2,1,0:T(4,128)(2,1)} %bitcast_dynamic-update-slice_fusion.6, bf16[128,4,256]{2,1,0:T(4,128)(2,1)} %param.13), kind=kLoop, calls=%fused_computation.61 | loop fusion | bytes 65536
  4.9 1.4 %bitcast_dynamic-update-slice_fusion.4 = bf16[8,16,4,256]{3,2,1,0:T(4,128)(2,1)} fusion(bf16[8,16,4,256]{3,2,1,0:T(4,128)(2,1)} %bitcast_dynamic-update-slice_fusion.5, bf16[128,4,256]{2,1,0:T(4,128)(2,1)} %param.13), kind=kLoop, calls=%fused_computation.60 | loop fusion | bytes 65536
  6.3 1.4 %bitcast_dynamic-update-slice_fusion.3 = bf16[8,16,4,256]{3,2,1,0:T(4,128)(2,1)} fusion(bf16[8,16,4,256]{3,2,1,0:T(4,128)(2,1)} %bitcast_dynamic-update-slice_fusion.4, bf16[128,4,256]{2,1,0:T(4,128)(2,1)} %param.13), kind=kLoop, calls=%fused_computation.59 | loop fusion | bytes 65536
  7.7 1.4 %bitcast_dynamic-update-slice_fusion.2 = bf16[8,16,4,256]{3,2,1,0:T(4,128)(2,1)} fusion(bf16[8,16,4,256]{3,2,1,0:T(4,128)(2,1)} %bitcast_dynamic-update-slice_fusion.3, bf16[128,4,256]{2,1,0:T(4,128)(2,1)} %param.13), kind=kLoop, calls=%fused_computation.58 | loop fusion | bytes 65536
  9.0 1.4 %bitcast_dynamic-update-slice_fusion.1 = bf16[8,16,4,256]{3,2,1,0:T(4,128)(2,1)} fusion(bf16[8,16,4,256]{3,2,1,0:T(4,128)(2,1)} %bitcast_dynamic-update-slice_fusion.2, bf16[128,4,256]{2,1,0:T(4,128)(2,1)} %param.13), kind=kLoop, calls=%fused_computation.57 | loop fusion | bytes 65536
  10.4 1.4 %bitcast_dynamic-update-slice_fusion = bf16[8,16,4,256]{3,2,1,0:T(4,128)(2,1)} fusion(bf16[8,16,4,256]{3,2,1,0:T(4,128)(2,1)} %bitcast_dynamic-update-slice_fusion.1, bf16[128,4,256]{2,1,0:T(4,128)(2,1)} %param.13), kind=kLoop, calls=%fused_computation.56 | loop fusion | bytes 65536 | tf_op jit(solution)/shard_map/stack | solution.py:29
  11.8 7.3 %all-to-all-start = ((bf16[8,16,4,256]{3,2,1,0:T(4,128)(2,1)}), bf16[8,16,4,256]{3,2,1,0:T(4,128)(2,1)S(1)}, u32[]{:S(2)}, u32[]{:S(2)}) async-start(bf16[8,16,4,256]{3,2,1,0:T(4,128)(2,1)} %bitcast_dynamic-update-slice_fusion), calls=%async_computation | async-start | bytes 524288 | tf_op jit(solution)/shard_map/all_to_all | solution.py:28
  20.3 0.8 multiply_add_fusion.9
  21.2 1.2 %broadcast_bitcast_fusion = f32[256]{0:T(256)} fusion(f32[128]{0:T(128)} %param.21), kind=kLoop, calls=%fused_computation.92 | loop fusion | bytes 1536 | tf_op jit(solution)/shard_map/mul | solution.py:75
  22.5 1.2 %broadcast_compare_fusion.3 = (pred[16]{0:T(512)(128)(4,1)}, pred[16]{0:T(512)(128)(4,1)}, pred[16]{0:T(512)(128)(4,1)}, pred[16]{0:T(512)(128)(4,1)}) fusion(s32[16]{0:T(128)} %param.25), kind=kLoop, calls=%fused_computation.98 | loop fusion | flops 64 | bytes 128 | tf_op jit(solution)/shard_map/gt | solution.py:57
  23.7 0.8 reshape.127
  25.1 7.1 %add_select_fusion = f32[16,2,128,128]{3,2,1,0:T(8,128)S(1)} fusion(f32[16,2,128,128]{3,2,1,0:T(8,128)} %param.22, f32[16,2,128]{2,1,0:T(2,128)} %get-tuple-element.29, f32[16,2,128]{2,1,0:T(2,128)S(1)} %get-tuple-element.25, f32[16,2,128]{2,1,0:T(2,128)} %get-tuple-element.27, f32[16,2,128]{2,1,0:T(2,128)S(1)} %get-tuple-element.24, ...), kind=kLoop, calls=%fused_computation.7 | loop fusion | flops 8388608 | bytes 4390976 | tf_op jit(solution)/shard_map/jit(_where)/select_n | solution.py:62
  32.7 1.1 %copy.37 = f32[16,4,8,256]{3,2,0,1:T(8,128)} copy(f32[16,4,8,256]{3,1,0,2:T(4,128)S(1)} %convert_bitcast_fusion) | data formatting | bytes 1048576 | tf_op jit(solution)/shard_map/convert_element_type | solution.py:36
  33.8 1.9 %reshape.125 = f32[16,4,2048]{2,0,1:T(8,128)} reshape(f32[16,4,8,256]{3,2,0,1:T(8,128)} %copy.37) | data formatting | bytes 1048576 | tf_op jit(solution)/shard_map/convert_element_type | solution.py:36
  35.7 1.2 %multiply_convert_fusion = bf16[16,4,2048]{2,0,1:T(8,128)(2,1)S(1)} fusion(f32[16,4,2048]{2,0,1:T(8,128)} %reshape.125, f32[2048]{0:T(1024)S(1)} %copy-done.5, f32[16,4]{0,1:T(4,128)S(1)} %add_rsqrt_fusion.1), kind=kLoop, calls=%fused_computation.46 | loop fusion | flops 393216 | bytes 794880 | tf_op jit(solution)/shard_map/convert_element_type | solution.py:38
  36.9 1.5 %fusion.14 = f32[16,4,256]{2,0,1:T(8,128)S(1)} fusion(bf16[16,4,2048]{2,0,1:T(8,128)(2,1)S(1)} %multiply_convert_fusion, bf16[2048,256]{1,0:T(8,128)(2,1)} %param.16, f32[256]{0:T(256)S(1)} %copy-done.4, f32[256]{0:T(256)S(1)} %copy-done.2), kind=kOutput, calls=%fused_computation.21 | convolution fusion | flops 67223552 | bytes 1378304 | tf_op jit(solution)/shard_map/dot_general | solution.py:42
  38.5 1.5 %fusion.7 = f32[16,4,256]{2,0,1:T(8,128)S(1)} fusion(bf16[16,4,2048]{2,0,1:T(8,128)(2,1)S(1)} %multiply_convert_fusion, bf16[2048,256]{1,0:T(8,128)(2,1)} %param.17), kind=kOutput, calls=%fused_computation.13 | convolution fusion | flops 67141632 | bytes 1376256 | tf_op jit(solution)/shard_map/dot_general | solution.py:43
  40.7 2.2 %divide_multiply_fusion = f32[16,4,256]{2,0,1:T(8,128)} fusion(bf16[16,4,2048]{2,0,1:T(8,128)(2,1)S(1)} %multiply_convert_fusion, bf16[2048,256]{1,0:T(8,128)(2,1)} %param.15), kind=kOutput, calls=%fused_computation.55 | convolution fusion | flops 67207168 | bytes 1376256 | tf_op jit(solution)/shard_map/dot_general | solution.py:41
  42.8 0.9 reshape.118
  44.6 2.8 %fusion.4 = f32[16,2,1,128]{3,2,1,0:T(1,128)S(1)} fusion(f32[16,2,128,1]{2,3,1,0:T(1,128)S(1)} %bitcast.158, f32[16,2,128,128]{3,2,1,0:T(8,128)S(1)} %add_select_fusion, f32[16,2,128]{2,1,0:T(2,128)S(1)} %get-tuple-element.14, f32[16,2,128]{2,1,0:T(2,128)S(1)} %get-tuple-element.10, f32[16,2,128]{2,1,0:T(2,128)S(1)} %get-tuple-element.37), kind=kOutput, calls=%fused_computation.8 | convolution fusion | flops 7864320 | bytes 2179072 | tf_op jit(solution)/shard_map/bhk,bhkv->bhv/dot_general | solution.py:71
  47.4 4.3 %fusion.36 = f32[16,2,1,128]{3,2,1,0:T(1,128)S(1)} fusion(f32[16,2,128,1]{2,3,1,0:T(1,128)S(1)} %bitcast.167, f32[16,2,128,128]{3,2,1,0:T(8,128)S(1)} %add_select_fusion, f32[16,2,128]{2,1,0:T(2,128)S(1)} %get-tuple-element.17, f32[16,2,128]{2,1,0:T(2,128)S(1)} %get-tuple-element.13, f32[16,2,128]{2,1,0:T(2,128)S(1)} %get-tuple-element.34, ...), kind=kOutput, calls=%fused_computation.47 | convolution fusion | flops 9437184 | bytes 2228224 | tf_op jit(solution)/shard_map/bhk,bhkv->bhv/dot_general | solution.py:71
  51.6 6.1 %fusion.5 = f32[16,2,1,128]{3,2,1,0:T(1,128)S(1)} fusion(f32[16,2,128,1]{2,3,1,0:T(1,128)S(1)} %bitcast.166, f32[16,2,128]{2,1,0:T(2,128)S(1)} %get-tuple-element.16, f32[16,2,128]{2,1,0:T(2,128)S(1)} %get-tuple-element.12, f32[16,2,128]{2,1,0:T(2,128)S(1)} %get-tuple-element.35, f32[16,2,128,128]{3,2,1,0:T(8,128)S(1)} %add_select_fusion, ...), kind=kOutput, calls=%fused_computation.9 | convolution fusion | flops 11010048 | bytes 2277376 | tf_op jit(solution)/shard_map/bhk,bhkv->bhv/dot_general | solution.py:71
  57.7 7.2 %fusion = f32[16,2,1,128]{3,2,1,0:T(1,128)S(1)} fusion(f32[16,2,128,1]{2,3,1,0:T(1,128)S(1)} %bitcast.165, f32[16,2,128]{2,1,0:T(2,128)S(1)} %get-tuple-element.15, f32[16,2,128]{2,1,0:T(2,128)S(1)} %get-tuple-element.11, f32[16,2,128]{2,1,0:T(2,128)S(1)} %get-tuple-element.36, f32[16,2,128]{2,1,0:T(2,128)S(1)} %get-tuple-element.16, ...), kind=kOutput, calls=%fused_computation | convolution fusion | flops 12582912 | bytes 2326528 | tf_op jit(solution)/shard_map/bhk,bhkv->bhv/dot_general | solution.py:71
  65.4 2.0 %fusion.16 = f32[16,4,2048]{2,0,1:T(8,128)S(1)} fusion(bf16[1024,2048]{1,0:T(8,128)(2,1)} %param.19, s32[]{:T(128)S(6)} %select_n.20, f32[16,4,256]{2,0,1:T(8,128)S(1)} %mul.343, f32[16,1,256]{2,0,1:T(8,128)S(1)} %stack.64, f32[16,1,256]{2,0,1:T(8,128)S(1)} %stack.63, f32[16,1,256]{2,0,1:T(8,128)S(1)} %stack.62, f32[16,1,256]{2,0,1:T(8,128)S(1)} %stack.61, ...), kind=kOutput, calls=%fused_computation.24 | convolution fusion | flops 134430720 | bytes 3015684 | tf_op jit(solution)/shard_map/dot_general | solution.py:81
  67.5 16.6 %all-reduce.1 = bf16[16,4,2048]{2,0,1:T(8,128)(2,1)S(1)} all-reduce(f32[16,4,2048]{2,0,1:T(8,128)S(1)} %fusion.16), channel_id=1, replica_groups=mesh['kv'=8,'tp'=4] {'tp'}, use_global_device_ids=true, to_apply=%region_2.3 | all-reduce | flops 131072 | bytes 786432 | tf_op jit(solution)/shard_map/psum | solution.py:82
  84.1 1.4 %copy.44 = bf16[16,4,2048]{0,1,2:T(4,128)(2,1)S(1)} copy(bf16[16,4,2048]{2,0,1:T(8,128)(2,1)S(1)} %all-reduce.1) | data formatting | bytes 524288 | tf_op jit(solution)/shard_map/convert_element_type | solution.py:82
  85.5 2.2 %reshape.144 = bf16[8,2,8192]{2,1,0:T(2,128)(2,1)S(1)} reshape(bf16[2048,4,16]{2,1,0:T(4,128)(2,1)S(1)} %bitcast.153) | data formatting | bytes 524288
  87.7 14.9 %all_to_all.23 = bf16[8,2,8192]{2,1,0:T(2,128)(2,1)} all-to-all(bf16[8,2,8192]{2,1,0:T(2,128)(2,1)S(1)} %reshape.144), channel_id=1, replica_groups=mesh['kv'=8,'tp'=4] {'kv'}, dimensions={0} | all-to-all | bytes 524288 | tf_op jit(solution)/shard_map/all_to_all | solution.py:83
  102.5 2.4 %reshape.145 = bf16[2048,4,16]{2,1,0:T(4,128)(2,1)S(1)} reshape(bf16[8,2,8192]{2,1,0:T(2,128)(2,1)} %all_to_all.23) | data formatting | bytes 524288
  104.9 2.0 %copy.45 = bf16[8,16,4,256]{3,2,1,0:T(4,128)(2,1)} copy(bf16[8,16,4,256]{1,2,3,0:T(4,128)(2,1)S(1)} %bitcast.154) | data formatting | bytes 524288 | tf_op jit(solution)/shard_map/all_to_all | solution.py:83
  (37 shorter events, 4.3 us)
Async XLA Ops:
  0.6 64.8 %copy-start = (bf16[2048,256]{1,0:T(8,128)(2,1)S(1)}, bf16[2048,256]{1,0:T(8,128)(2,1)}, u32[]{:S(2)}) copy-start(bf16[2048,256]{1,0:T(8,128)(2,1)} %param.18) | copy-start | bytes 3145732
  11.8 20.5 %all-to-all-start = ((bf16[8,16,4,256]{3,2,1,0:T(4,128)(2,1)}), bf16[8,16,4,256]{3,2,1,0:T(4,128)(2,1)S(1)}, u32[]{:S(2)}, u32[]{:S(2)}) async-start(bf16[8,16,4,256]{3,2,1,0:T(4,128)(2,1)} %bitcast_dynamic-update-slice_fusion), calls=%async_computation | async-start | bytes 524288 | tf_op jit(solution)/shard_map/all_to_all | solution.py:28
  19.8 0.6 copy-start.3
  32.3 25.5 %copy-start.1 = (f32[16,2,128,128]{3,2,1,0:T(8,128)}, f32[16,2,128,128]{3,2,1,0:T(8,128)S(1)}, u32[]{:S(2)}) copy-start(f32[16,2,128,128]{3,2,1,0:T(8,128)S(1)} %add_select_fusion) | copy-start | bytes 6291460
  32.3 3.5 %copy-start.5 = (f32[2048]{0:T(1024)S(1)}, f32[2048]{0:T(1024)}, u32[]{:S(2)}) copy-start(f32[2048]{0:T(1024)} %param.14) | copy-start | bytes 24580
  32.3 4.6 %copy-start.2 = (f32[256]{0:T(256)S(1)}, f32[256]{0:T(256)}, u32[]{:S(2)}) copy-start(f32[256]{0:T(256)} %param.20) | copy-start | bytes 3076
  32.3 4.6 %copy-start.4 = (f32[256]{0:T(256)S(1)}, f32[256]{0:T(256)}, u32[]{:S(2)}) copy-start(f32[256]{0:T(256)} %copy-done.3) | copy-start | bytes 3076
  57.7 7.7 %copy-start.6 = (f32[256]{0:T(256)S(1)}, f32[256]{0:T(256)}, u32[]{:S(2)}) copy-start(f32[256]{0:T(256)} %broadcast_bitcast_fusion) | copy-start | bytes 3076
